TPU v7x, 32 devices: a whole 2x2x4 slice. The times are simulated.
32 devices in a mesh: gr: 2 (over y), sp: 4 (over z), tp: 4 (over x, core).
Axes of the slice: x: 2, y: 2, z: 4, core: 2. Of those that a mesh axis runs over, the one named last changes fastest.
Arguments:
- tokens: bfloat16 [4, 1024, 4096], P('gr', ('sp', 'tp')), parts along dimension 0, may hold values from -6 to 6
- norm_gain: bfloat16 [4096], replicated, may hold values from 0.099609375 to 1.8984375
- key_weight: bfloat16 [4096, 1024], P(None, 'tp'), may hold values from -0.09375 to 0.09375
- value_weight: bfloat16 [4096, 1024], P(None, 'tp'), may hold values from -0.09375 to 0.09375
- cum_gates: float32 [4, 1024, 16], P('gr', 'sp', 'tp'), parts along dimension 0, may hold values from -173 to 0, as said below
- new_query: bfloat16 [4, 1024], P('gr', 'tp'), parts along dimension 0, may hold values from -240 to 240
- new_key: bfloat16 [4, 1024], P('gr', 'tp'), parts along dimension 0, may hold values from -6 to 6
- new_value: bfloat16 [4, 1024], P('gr', 'tp'), parts along dimension 0, may hold values from -6 to 6
- new_gate: float32 [4, 16], P('gr', 'tp'), parts along dimension 0, may hold values from -5 to -1.5
Outputs:
- key_cache: bfloat16 [4, 1024, 1024], P('gr', 'sp', 'tp'), parts along dimension 0
- value_cache: bfloat16 [4, 1024, 1024], P('gr', 'sp', 'tp'), parts along dimension 0
- readout: bfloat16 [4, 1024], P('gr', 'tp'), parts along dimension 0
There are 2 independent parts, one for each index of `gr`. A program takes and returns all parts, laid end to end along the dimension named above; an argument that names none is the same for every part. Nothing has to cross between parts.
Inputs may be any that keep to these rules, and one draw needn't show every extreme that they name: `cum_gates`: along positions, for each prompt and head, the values never rise.
All inputs are finite; a program needn't handle non-finite values.
Results may differ from a plain program's by a relative error of at most 0.005.
The roundings to bfloat16 on the way count: a program that leaves them out, or rounds other values in their place, can miss the bound.
Values may be sent and summed in bfloat16 or wider, within the bound.
A program may use at most 64 MiB of HBM per device.

v0:
```python
import jax
import jax.numpy as jnp
from jax import lax
from jax.sharding import PartitionSpec as P

HD = 64
epsilon = 1e-06
masked_score = -1e30


def body(
    tokens, norm_gain, key_weight, value_weight, cum_gates, new_query, new_key, new_value, new_gate
):
    seq_count, own_len, model_width = tokens.shape
    as_float = tokens.astype(jnp.float32)
    normed = (
        as_float
        * lax.rsqrt(jnp.mean(as_float * as_float, axis=-1, keepdims=True) + epsilon)
        * norm_gain.astype(jnp.float32)
    ).astype(jnp.bfloat16)
    key_width = key_weight.shape[1]
    local_heads = key_width // HD
    both_weights = jnp.concatenate([key_weight, value_weight], axis=1)
    piece = lax.all_gather(normed, "tp", axis=1, tiled=True)
    piece_len = piece.shape[1]
    rows = piece.reshape(seq_count * piece_len, model_width)
    result = jnp.dot(rows, both_weights, preferred_element_type=jnp.float32).astype(jnp.bfloat16)
    projected = result.reshape(seq_count, piece_len, 2 * key_width)
    key_cache = projected[:, :, :key_width]
    value_cache = projected[:, :, key_width:]
    block_len = projected.shape[1]
    sp_count = lax.axis_size("sp")
    sp_index = lax.axis_index("sp")
    score_scale = HD ** (-0.5)
    queries = new_query.reshape(seq_count, local_heads, HD)
    fresh_key = new_key.reshape(seq_count, local_heads, HD).astype(jnp.float32)
    fresh_value = new_value.reshape(seq_count, local_heads, HD).astype(jnp.float32)
    fresh_score = jnp.sum(queries.astype(jnp.float32) * fresh_key, axis=-1) * score_scale
    key_heads = key_cache.reshape(seq_count, block_len, local_heads, HD)
    value_heads = value_cache.reshape(seq_count, block_len, local_heads, HD).astype(jnp.float32)
    scores = (
        jnp.einsum("shd,slhd->shl", queries, key_heads, preferred_element_type=jnp.float32)
        * score_scale
    )
    scores = scores - jnp.transpose(cum_gates, (0, 2, 1))
    last_block = sp_index == sp_count - 1
    fresh_term = jnp.where(
        last_block, fresh_score - (cum_gates[:, block_len - 1, :] + new_gate), masked_score
    )
    local_top = jnp.maximum(jnp.max(scores, axis=-1), fresh_term)
    maxima = lax.pmax(local_top, "sp")
    weights = jnp.exp(scores - maxima[:, :, None])
    fresh_weight = jnp.exp(fresh_term - maxima)
    totals = jnp.sum(weights, axis=-1) + fresh_weight
    weighted = jnp.einsum("shl,slhd->shd", weights, value_heads, precision=lax.Precision.HIGHEST)
    weighted = weighted + fresh_weight[:, :, None] * fresh_value
    totals, weighted = lax.psum((totals, weighted), "sp")
    readout = (weighted / totals[:, :, None]).reshape(seq_count, key_width).astype(jnp.bfloat16)
    return (key_cache, value_cache, readout)


def solution(mesh):
    in_specs = (
        P("gr", ("sp", "tp"), None),
        P(),
        P(None, "tp"),
        P(None, "tp"),
        P("gr", "sp", "tp"),
        P("gr", "tp"),
        P("gr", "tp"),
        P("gr", "tp"),
        P("gr", "tp"),
    )
    out_specs = (P("gr", "sp", "tp"), P("gr", "sp", "tp"), P("gr", "tp"))
    return jax.shard_map(body, mesh=mesh, in_specs=in_specs, out_specs=out_specs, check_vma=False)
```

profile of v0, /device:TPU:0, one launch (start us, length us, event | category | flops | bytes accessed | tf_op | source)
XLA Modules:
  0.0 83.7 jit_solution(6548077247722289311)
XLA Ops:
  7.2 0.0 all-gather.2.cloned.1.call-start
  7.2 0.7 convert_element_type.35
  7.9 1.7 %fusion.4 = f32[2,64]{1,0:T(2,128)S(1)} fusion(bf16[2,64,4096]{2,1,0:T(8,128)(2,1)} %param.9), kind=kLoop, calls=%fused_computation.6 | loop fusion | flops 1572736 | bytes 1049088 | tf_op jit(solution)/shard_map/reduce_sum | solution.py:18
  9.6 2.5 %fusion.6 = bf16[2,64,4096]{2,1,0:T(8,128)(2,1)} fusion(bf16[2,64,4096]{2,1,0:T(8,128)(2,1)} %param.9, f32[4096]{0:T(1024)S(1)} %convert_element_type.35, f32[2,64]{1,0:T(2,128)S(1)} %add_rsqrt_fusion), kind=kLoop, calls=%fused_computation.8 | loop fusion | flops 2097152 | bytes 2114048 | tf_op jit(solution)/shard_map/convert_element_type | solution.py:20
  12.2 0.0 all-gather.2.cloned.1.call-update
  12.2 0.1 reshape.53
  12.3 0.1 reshape.44
  12.4 0.1 reshape.46
  12.4 0.1 reshape.47
  12.5 0.2 slice_reduce_fusion
  12.7 0.1 multiply_reduce_fusion
  12.8 36.7 %all-gather.2.cloned.1.call-done = bf16[2,256,4096]{2,1,0:T(8,128)(2,1)} async-done(((bf16[2,64,4096]{2,1,0:T(8,128)(2,1)}), bf16[2,256,4096]{2,1,0:T(8,128)(2,1)}) %all-gather.2.cloned.1.call-update) | async-done | bytes 4194320 | tf_op jit(solution)/shard_map/all_gather | solution.py:24
  49.5 5.2 %fusion.7 = bf16[512,512]{1,0:T(8,128)(2,1)S(1)} fusion(bf16[512,4096]{1,0:T(8,128)(2,1)} %bitcast.34, bf16[4096,256]{1,0:T(8,128)(2,1)S(1)} %copy-done.7, bf16[4096,256]{1,0:T(8,128)(2,1)} %param.11), kind=kOutput, calls=%fused_computation.9 | convolution fusion | flops 2156134400 | bytes 8912896 | tf_op jit(solution)/shard_map/dot_general | solution.py:27
  54.8 0.1 copy.20
  55.0 0.1 fusion.19
  55.1 0.1 fusion.15
  55.2 11.7 %pmax.7 = f32[2,4]{1,0:T(2,128)S(1)} all-reduce(f32[2,4]{1,0:T(2,128)S(1)} %get-tuple-element.10), channel_id=1, replica_groups=mesh['gr'=2,'sp'=4,'tp'=4] {'sp'}, use_global_device_ids=true, to_apply=%region_3.4 | all-reduce | flops 8 | bytes 64 | tf_op jit(solution)/shard_map/pmax | solution.py:51
  66.9 0.2 fusion.12
  67.1 0.1 copy.21
  67.2 0.3 fusion.10
  67.5 0.1 multiply_add_fusion
  67.6 8.5 %all-reduce = (f32[2,4,64]{2,1,0:T(4,128)S(1)}, f32[2,4]{1,0:T(2,128)S(1)}) all-reduce(f32[2,4,64]{2,1,0:T(4,128)S(1)} %multiply_add_fusion, f32[2,4]{1,0:T(2,128)S(1)} %get-tuple-element.8), channel_id=1, replica_groups=mesh['gr'=2,'sp'=4,'tp'=4] {'sp'}, use_global_device_ids=true, to_apply=%region_4.5 | all-reduce | flops 520 | bytes 4160 | tf_op jit(solution)/shard_map/psum | solution.py:57
  76.1 0.1 divide_convert_fusion
  76.2 0.7 convert_element_type.44
  (20 shorter events, 0.1 us)
Async XLA Ops:
  7.2 42.3 %all-gather.2.cloned.1.call-start = ((), (), s32[]{:S(2)}) async-start(), calls=%async_computation | async-start | bytes 5242880 | tf_op jit(solution)/shard_map/all_gather | solution.py:24
  7.9 4.3 %copy-start.3 = (bf16[2,256]{1,0:T(2,128)(2,1)S(1)}, bf16[2,256]{1,0:T(2,128)(2,1)}, u32[]{:S(2)}) copy-start(bf16[2,256]{1,0:T(2,128)(2,1)} %param.14) | copy-start | bytes 3076
  7.9 4.4 %copy-start.4 = (bf16[2,256]{1,0:T(2,128)(2,1)S(1)}, bf16[2,256]{1,0:T(2,128)(2,1)}, u32[]{:S(2)}) copy-start(bf16[2,256]{1,0:T(2,128)(2,1)} %param.15) | copy-start | bytes 3076
  7.9 4.5 %copy-start.5 = (bf16[2,256]{1,0:T(2,128)(2,1)S(1)}, bf16[2,256]{1,0:T(2,128)(2,1)}, u32[]{:S(2)}) copy-start(bf16[2,256]{1,0:T(2,128)(2,1)} %param.16) | copy-start | bytes 3076
  7.9 4.6 %copy-start.2 = (f32[2,256,4]{1,2,0:T(4,128)S(1)}, f32[2,256,4]{1,2,0:T(4,128)}, u32[]{:S(2)}) copy-start(f32[2,256,4]{1,2,0:T(4,128)} %param.13) | copy-start | bytes 24580
  7.9 41.6 %copy-start.7 = (bf16[4096,256]{1,0:T(8,128)(2,1)S(1)}, bf16[4096,256]{1,0:T(8,128)(2,1)}, u32[]{:S(2)}) copy-start(bf16[4096,256]{1,0:T(8,128)(2,1)} %param.12) | copy-start | bytes 6291460
  49.5 5.7 %copy-start.6 = (f32[2,4]{1,0:T(2,128)S(1)}, f32[2,4]{1,0:T(2,128)}, u32[]{:S(2)}) copy-start(f32[2,4]{1,0:T(2,128)} %param.17) | copy-start | bytes 100
  54.8 22.1 %copy-start = (bf16[2,256,256]{2,1,0:T(8,128)(2,1)}, bf16[2,256,256]{2,1,0:T(8,128)(2,1)S(1)}, u32[]{:S(2)}) copy-start(bf16[2,256,256]{2,1,0:T(8,128)(2,1)S(1)} %get-tuple-element.12) | copy-start | bytes 786436
  54.8 22.0 %copy-start.1 = (bf16[2,256,256]{2,1,0:T(8,128)(2,1)}, bf16[2,256,256]{2,1,0:T(8,128)(2,1)S(1)}, u32[]{:S(2)}) copy-start(bf16[2,256,256]{2,1,0:T(8,128)(2,1)S(1)} %get-tuple-element.13) | copy-start | bytes 786436
Sparse Core Ops, SparseCore 0:
  12.3 37.1 all-gather.1
where the time goes:
time: 84 us; the launch traced here: 83.7 us
  waiting for transfers between devices  36.8 us (44%)
  blocking collectives  20.2 us (24%)
  between operations  14.1 us (17%)
  matrix products  5.69 us (7%)
  other arithmetic  5.42 us (6%)
  local copies, waits for them, and re-layouts  1.48 us (2%)
    all_gather x1, waiting for transfers between devices, body(): piece = lax.all_gather(normed, 'tp', axis=1, tiled=True)  36.7 us
    pmax x1, blocking collectives, body(): maxima = lax.pmax(local_top, 'sp')  11.7 us
    psum x1, blocking collectives, body(): totals, weighted = lax.psum((totals, weighted), 'sp')  8.5 us
    dot_general x1, matrix products, body(): jnp.dot(rows, both_weights, preferred_element_type=jnp.float32)  5.24 us
    convert_element_type x1, other arithmetic, body(): normed = (as_float * lax.rsqrt(jnp.mean(as_float * as_float, axis=-1, kee...  2.53 us
  transfers between devices with their start and end apart: 1, of which 1 were waited for; matrix products, arithmetic and copies ran while one was open for 1% of the time, Pallas kernels for 0%

commit v1 on v0

--- a/solution.py
+++ b/solution.py
@@ -21,7 +21,9 @@
     key_width = key_weight.shape[1]
     local_heads = key_width // HD
     both_weights = jnp.concatenate([key_weight, value_weight], axis=1)
-    piece = lax.all_gather(normed, "tp", axis=1, tiled=True)
+    piece = jnp.concatenate(
+        lax.all_to_all(jnp.stack([normed] * lax.axis_size("tp")), "tp", 0, 0), axis=1
+    )
     piece_len = piece.shape[1]
     rows = piece.reshape(seq_count * piece_len, model_width)
     result = jnp.dot(rows, both_weights, preferred_element_type=jnp.float32).astype(jnp.bfloat16)

time: 84 us -> 89.5 us (1.065)
  between operations: 14.1 us -> 0.75 us
  waiting for transfers between devices: 36.8 us -> 48.3 us
  local copies, waits for them, and re-layouts: 1.48 us -> 6.8 us
  starting transfers between devices: 0.04 us -> 5 us
  matrix products: 5.69 us -> 2.77 us
  other arithmetic: 5.42 us -> 4.29 us
  blocking collectives: 20.2 us -> 21.3 us
    all_to_all x0 -> x1, waiting for transfers between devices: none -> 48.3 us  [body(): lax.all_to_all(jnp.stack([normed] * lax.axis_size('tp')), 'tp', 0, 0)]
    all_gather x1 -> x0, waiting for transfers between devices: 36.7 us -> none  [body(): piece = lax.all_gather(normed, 'tp', axis=1, tiled=True)]
    all_to_all x0 -> x1, starting transfers between devices: none -> 5 us  [body(): lax.all_to_all(jnp.stack([normed] * lax.axis_size('tp')), 'tp', 0, 0)]
    dot_general x1, matrix products: 5.24 us -> 2.32 us  [body(): jnp.dot(rows, both_weights, preferred_element_type=jnp.float32)]
    all_to_all x0 -> x1, local copies, waits for them, and re-layouts: none -> 2.61 us  [body(): lax.all_to_all(jnp.stack([normed] * lax.axis_size('tp')), 'tp', 0, 0)]
    another operation x0 -> x1, local copies, waits for them, and re-layouts: none -> 2.48 us  [body(): jnp.stack([normed] * lax.axis_size('tp'))]
    pmax x1, blocking collectives: 11.7 us -> 12.8 us  [body(): maxima = lax.pmax(local_top, 'sp')]
    convert_element_type x1, other arithmetic: 2.53 us -> 1.55 us  [body(): normed = (as_float * lax.rsqrt(jnp.mean(as_float * as_float, axis=-1, kee...]
where the time goes in v1:
time: 89.5 us; the launch traced here: 89.2 us
  waiting for transfers between devices  48.3 us (54%)
  blocking collectives  21.3 us (24%)
  local copies, waits for them, and re-layouts  6.8 us (8%)
  starting transfers between devices  5 us (6%)
  other arithmetic  4.29 us (5%)
  matrix products  2.77 us (3%)
    all_to_all x1, waiting for transfers between devices, body(): lax.all_to_all(jnp.stack([normed] * lax.axis_size('tp')), 'tp', 0, 0)  48.3 us
    pmax x1, blocking collectives, body(): maxima = lax.pmax(local_top, 'sp')  12.8 us
    psum x1, blocking collectives, body(): totals, weighted = lax.psum((totals, weighted), 'sp')  8.5 us
    all_to_all x1, starting transfers between devices, body(): lax.all_to_all(jnp.stack([normed] * lax.axis_size('tp')), 'tp', 0, 0)  5 us
    all_to_all x1, local copies, waits for them, and re-layouts, body(): lax.all_to_all(jnp.stack([normed] * lax.axis_size('tp')), 'tp', 0, 0)  2.61 us
    another operation x1, local copies, waits for them, and re-layouts, body(): jnp.stack([normed] * lax.axis_size('tp'))  2.48 us
    dot_general x1, matrix products, body(): jnp.dot(rows, both_weights, preferred_element_type=jnp.float32)  2.32 us
  transfers between devices with their start and end apart: 1, of which 1 were waited for; matrix products, arithmetic and copies ran while one was open for 1% of the time, Pallas kernels for 0%

profile of v1, /device:TPU:0, one launch (start us, length us, event | category | flops | bytes accessed | tf_op | source)
XLA Modules:
  0.0 89.2 jit_solution(17260342584295695094)
XLA Ops:
  0.6 0.7 convert_element_type.35
  1.3 1.5 %fusion.4 = f32[2,64]{1,0:T(2,128)S(1)} fusion(bf16[2,64,4096]{2,1,0:T(8,128)(2,1)} %param.9), kind=kLoop, calls=%fused_computation.6 | loop fusion | flops 1572736 | bytes 1049088 | tf_op jit(solution)/shard_map/reduce_sum | solution.py:18
  2.9 1.6 %fusion.6 = bf16[2,64,4096]{2,1,0:T(8,128)(2,1)S(1)} fusion(bf16[2,64,4096]{2,1,0:T(8,128)(2,1)} %param.9, f32[4096]{0:T(1024)S(1)} %convert_element_type.35, f32[2,64]{1,0:T(2,128)S(1)} %add_rsqrt_fusion), kind=kLoop, calls=%fused_computation.8 | loop fusion | flops 2097152 | bytes 2114048 | tf_op jit(solution)/shard_map/convert_element_type | solution.py:20
  4.4 2.5 %stack.2 = bf16[4,2,64,4096]{3,2,1,0:T(8,128)(2,1)} broadcast(bf16[2,64,4096]{2,1,0:T(8,128)(2,1)S(1)} %fusion.6), dimensions={1,2,3} | broadcast | bytes 5242880 | tf_op jit(solution)/shard_map/stack | solution.py:25
  6.9 5.0 %all-to-all-start = ((bf16[4,2,64,4096]{3,2,1,0:T(8,128)(2,1)}), bf16[4,2,64,4096]{3,2,1,0:T(8,128)(2,1)}, u32[]{:S(2)}, u32[]{:S(2)}) async-start(bf16[4,2,64,4096]{3,2,1,0:T(8,128)(2,1)} %stack.2), calls=%async_computation | async-start | bytes 8388608 | tf_op jit(solution)/shard_map/all_to_all | solution.py:25
  11.9 0.1 reshape.55
  12.0 0.1 reshape.46
  12.1 0.1 reshape.48
  12.2 0.1 reshape.49
  12.3 0.2 slice_reduce_fusion
  12.4 0.1 multiply_reduce_fusion
  12.5 48.3 %all-to-all-done = bf16[4,2,64,4096]{3,2,1,0:T(8,128)(2,1)} async-done(((bf16[4,2,64,4096]{3,2,1,0:T(8,128)(2,1)}), bf16[4,2,64,4096]{3,2,1,0:T(8,128)(2,1)}, u32[]{:S(2)}, u32[]{:S(2)}) %all-to-all-start) | async-done | bytes 4194336 | tf_op jit(solution)/shard_map/all_to_all | solution.py:25
  60.8 2.6 %copy.16 = bf16[4,2,64,4096]{3,2,0,1:T(8,128)(2,1)S(1)} copy(bf16[4,2,64,4096]{3,2,1,0:T(8,128)(2,1)} %all-to-all-done) | data formatting | bytes 8388608 | tf_op jit(solution)/shard_map/all_to_all | solution.py:25
  63.4 0.2 copy-done.8
  63.6 2.3 %fusion.7 = bf16[512,512]{1,0:T(8,128)(2,1)S(1)} fusion(bf16[512,4096]{1,0:T(8,128)(2,1)S(1)} %bitcast.32, bf16[4096,256]{1,0:T(8,128)(2,1)S(1)} %copy-done.7, bf16[4096,256]{1,0:T(8,128)(2,1)S(1)} %copy-done.8), kind=kOutput, calls=%fused_computation.9 | convolution fusion | flops 2156134400 | bytes 8912896 | tf_op jit(solution)/shard_map/dot_general | solution.py:29
  66.0 0.1 copy.25
  66.2 0.1 fusion.19
  66.3 0.1 fusion.15
  66.4 12.8 %pmax.7 = f32[2,4]{1,0:T(2,128)S(1)} all-reduce(f32[2,4]{1,0:T(2,128)S(1)} %get-tuple-element.13), channel_id=1, replica_groups=mesh['gr'=2,'sp'=4,'tp'=4] {'sp'}, use_global_device_ids=true, to_apply=%region_3.4 | all-reduce | flops 8 | bytes 64 | tf_op jit(solution)/shard_map/pmax | solution.py:53
  79.2 0.2 fusion.12
  79.4 0.1 copy.26
  79.5 0.3 fusion.10
  79.9 8.5 %all-reduce = (f32[2,4,64]{2,1,0:T(4,128)S(1)}, f32[2,4]{1,0:T(2,128)S(1)}) all-reduce(f32[2,4,64]{2,1,0:T(4,128)S(1)} %multiply_add_fusion, f32[2,4]{1,0:T(2,128)S(1)} %get-tuple-element.11), channel_id=1, replica_groups=mesh['gr'=2,'sp'=4,'tp'=4] {'sp'}, use_global_device_ids=true, to_apply=%region_4.5 | all-reduce | flops 520 | bytes 4160 | tf_op jit(solution)/shard_map/psum | solution.py:59
  88.5 0.7 convert_element_type.44
  (23 shorter events, 0.2 us)
Async XLA Ops:
  6.9 5.0 %copy-start.3 = (bf16[2,256]{1,0:T(2,128)(2,1)S(1)}, bf16[2,256]{1,0:T(2,128)(2,1)}, u32[]{:S(2)}) copy-start(bf16[2,256]{1,0:T(2,128)(2,1)} %param.14) | copy-start | bytes 3076
  6.9 5.2 %copy-start.4 = (bf16[2,256]{1,0:T(2,128)(2,1)S(1)}, bf16[2,256]{1,0:T(2,128)(2,1)}, u32[]{:S(2)}) copy-start(bf16[2,256]{1,0:T(2,128)(2,1)} %param.15) | copy-start | bytes 3076
  6.9 5.3 %copy-start.5 = (bf16[2,256]{1,0:T(2,128)(2,1)S(1)}, bf16[2,256]{1,0:T(2,128)(2,1)}, u32[]{:S(2)}) copy-start(bf16[2,256]{1,0:T(2,128)(2,1)} %param.16) | copy-start | bytes 3076
  6.9 5.4 %copy-start.2 = (f32[2,256,4]{1,2,0:T(4,128)S(1)}, f32[2,256,4]{1,2,0:T(4,128)}, u32[]{:S(2)}) copy-start(f32[2,256,4]{1,2,0:T(4,128)} %param.13) | copy-start | bytes 24580
  6.9 53.9 %all-to-all-start = ((bf16[4,2,64,4096]{3,2,1,0:T(8,128)(2,1)}), bf16[4,2,64,4096]{3,2,1,0:T(8,128)(2,1)}, u32[]{:S(2)}, u32[]{:S(2)}) async-start(bf16[4,2,64,4096]{3,2,1,0:T(8,128)(2,1)} %stack.2), calls=%async_computation | async-start | bytes 8388608 | tf_op jit(solution)/shard_map/all_to_all | solution.py:25
  12.5 50.9 %copy-start.7 = (bf16[4096,256]{1,0:T(8,128)(2,1)S(1)}, bf16[4096,256]{1,0:T(8,128)(2,1)}, u32[]{:S(2)}) copy-start(bf16[4096,256]{1,0:T(8,128)(2,1)} %param.12) | copy-start | bytes 6291460
  60.8 2.9 %copy-start.8 = (bf16[4096,256]{1,0:T(8,128)(2,1)S(1)}, bf16[4096,256]{1,0:T(8,128)(2,1)}, u32[]{:S(2)}) copy-start(bf16[4096,256]{1,0:T(8,128)(2,1)} %param.11) | copy-start | bytes 6291460
  63.6 2.8 %copy-start.6 = (f32[2,4]{1,0:T(2,128)S(1)}, f32[2,4]{1,0:T(2,128)}, u32[]{:S(2)}) copy-start(f32[2,4]{1,0:T(2,128)} %param.17) | copy-start | bytes 100
  66.0 23.1 %copy-start = (bf16[2,256,256]{2,1,0:T(8,128)(2,1)}, bf16[2,256,256]{2,1,0:T(8,128)(2,1)S(1)}, u32[]{:S(2)}) copy-start(bf16[2,256,256]{2,1,0:T(8,128)(2,1)S(1)} %get-tuple-element.15) | copy-start | bytes 786436
  66.0 23.1 %copy-start.1 = (bf16[2,256,256]{2,1,0:T(8,128)(2,1)}, bf16[2,256,256]{2,1,0:T(8,128)(2,1)S(1)}, u32[]{:S(2)}) copy-start(bf16[2,256,256]{2,1,0:T(8,128)(2,1)S(1)} %get-tuple-element.16) | copy-start | bytes 786436
